TPU v7x, 32 devices: a whole 2x2x4 slice. The times are simulated.
32 devices in a mesh: fs: 16 (over z, y, x), tp: 2 (over core).
Axes of the slice: x: 2, y: 2, z: 4, core: 2. Of those that a mesh axis runs over, the one named last changes fastest.
Arguments:
- prompt: bfloat16 [5120, 2048], P('fs', 'tp'), may hold values from -6 to 6
- norm_gain: float32 [2048], P('fs'), may hold values from 0.1 to 1.9
- gate_master: float32 [2048, 3072], P('fs', 'tp'), may hold values from -0.125 to 0.125
- up_master: float32 [2048, 3072], P('fs', 'tp'), may hold values from -0.125 to 0.125
- down_master: float32 [2048, 3072], P('fs', 'tp'), may hold values from -0.109375 to 0.109375
Outputs:
- gate_new: bfloat16 [3072, 2048], P('tp')
- up_new: bfloat16 [3072, 2048], P('tp')
- down_new: bfloat16 [3072, 2048], P('tp')
- mixed: bfloat16 [2048, 5120], P('tp', 'fs')
All inputs are finite; a program needn't handle non-finite values.
Results may differ from a plain program's by a relative error of at most 0.0082.
Values may be sent and summed in bfloat16 or wider, within the bound.
A program may use at most 128 MiB of HBM per device.

v0:
```python
import jax
import jax.numpy as jnp
from jax import lax
from jax.sharding import PartitionSpec as P


def on_device(prompt, norm_gain, gate_master, up_master, down_master):
    gain_col = norm_gain[:, None]
    gate_low = (gate_master * gain_col).astype(jnp.bfloat16).T
    up_low = (up_master * gain_col).astype(jnp.bfloat16).T
    down_low = down_master.astype(jnp.bfloat16).T
    whole = lax.all_gather(prompt, "tp", axis=1, tiled=True)
    values = whole.astype(jnp.float32)
    normed = (values * lax.rsqrt(jnp.mean(values * values, axis=1, keepdims=True) + 1e-06)).astype(
        jnp.bfloat16
    )
    contract = (((1,), (1,)), ((), ()))
    gate_new, up_new, down_new = (
        lax.all_gather(gate_low, "fs", axis=1, tiled=True),
        lax.all_gather(up_low, "fs", axis=1, tiled=True),
        lax.all_gather(down_low, "fs", axis=1, tiled=True),
    )
    gate = lax.dot_general(normed, gate_new, contract, preferred_element_type=jnp.float32)
    up = lax.dot_general(normed, up_new, contract, preferred_element_type=jnp.float32)
    hidden = (jax.nn.silu(gate) * up).astype(jnp.bfloat16)
    mixed = lax.psum_scatter(
        lax.dot_general(
            down_new, hidden, (((0,), (1,)), ((), ())), preferred_element_type=jnp.float32
        ),
        "tp",
        scatter_dimension=0,
        tiled=True,
    )
    return (gate_new, up_new, down_new, mixed.astype(jnp.bfloat16))


def solution(mesh):
    placed = (P("fs", "tp"), P("fs"), P("fs", "tp"), P("fs", "tp"), P("fs", "tp"))
    return jax.shard_map(
        on_device,
        mesh=mesh,
        in_specs=placed,
        out_specs=(P("tp", None), P("tp", None), P("tp", None), P("tp", "fs")),
        check_vma=False,
    )
```

profile of v0, /device:TPU:0, one launch (start us, length us, event | category | flops | bytes accessed | tf_op | source)
XLA Modules:
  0.0 414.9 jit_solution(16847187545937609317)
XLA Ops:
  7.2 0.0 all-gather.11.cloned.1.call-start
  7.2 0.7 all-gather.11.cloned.1.call-update
  7.9 0.0 all-gather.5.cloned.1.call-start
  8.0 1.4 copy.10
  9.4 0.3 copy.9
  9.7 1.0 fusion.8
  10.7 0.0 all-gather.7.cloned.1.call-start
  10.7 0.7 all-gather.7.cloned.1.call-update
  11.4 0.0 all-gather.9.cloned.1.call-start
  11.5 0.9 copy.11
  12.4 0.0 reduce-scatter.2.cloned.1.call-start
  12.5 9.2 %all-gather.11.cloned.1.call-done = bf16[320,2048]{1,0:T(8,128)(2,1)} async-done(((bf16[320,1024]{1,0:T(8,128)(2,1)}), bf16[320,2048]{1,0:T(8,128)(2,1)}) %all-gather.11.cloned.1.call-update) | async-done | bytes 1310736 | tf_op jit(solution)/shard_map/all_gather | solution.py:12
  21.7 1.7 fusion.1
  23.4 117.8 %all-gather.5.cloned.1.call-done = bf16[1536,2048]{1,0:T(8,128)(2,1)} async-done(((bf16[1536,128]{1,0:T(8,128)(2,1)}), bf16[1536,2048]{1,0:T(8,128)(2,1)}) %all-gather.5.cloned.1.call-update) | async-done | bytes 6291472 | tf_op jit(solution)/shard_map/all_gather | solution.py:19
  141.2 5.4 %fusion.5 = f32[320,1536]{1,0:T(8,128)S(1)} fusion(bf16[1536,2048]{1,0:T(8,128)(2,1)} %all-gather.5.cloned.1.call-done, bf16[320,2048]{1,0:T(8,128)(2,1)} %all-gather.11.cloned.1.call-done, f32[320]{0:T(512)S(1)} %add_rsqrt_fusion), kind=kOutput, calls=%fused_computation.9 | convolution fusion | flops 2015232000 | bytes 9569536 | tf_op jit(solution)/shard_map/dot_general | solution.py:23
  146.6 111.1 %all-gather.7.cloned.1.call-done = bf16[1536,2048]{1,0:T(8,128)(2,1)} async-done(((bf16[1536,128]{1,0:T(8,128)(2,1)}), bf16[1536,2048]{1,0:T(8,128)(2,1)}) %all-gather.7.cloned.1.call-update) | async-done | bytes 6291472 | tf_op jit(solution)/shard_map/all_gather | solution.py:20
  257.7 116.4 %all-gather.9.cloned.1.call-done = bf16[1536,2048]{1,0:T(8,128)(2,1)} async-done(((bf16[1536,128]{1,0:T(8,128)(2,1)}), bf16[1536,2048]{1,0:T(8,128)(2,1)}) %all-gather.9.cloned.1.call-update) | async-done | bytes 6291472 | tf_op jit(solution)/shard_map/all_gather | solution.py:21
  374.1 10.6 %convolution_bitcast_fusion = f32[2048,320]{0,1:T(8,128)} fusion(bf16[1536,2048]{1,0:T(8,128)(2,1)} %all-gather.9.cloned.1.call-done, bf16[1536,2048]{1,0:T(8,128)(2,1)} %all-gather.7.cloned.1.call-done, f32[320,1536]{1,0:T(8,128)S(1)} %fusion.5, bf16[320,2048]{1,0:T(8,128)(2,1)S(1)} %copy-done, f32[320]{0:T(512)S(1)} %add_rsqrt_fusion), kind=kOutput, calls=%fused_computation.3 | convolution fusion | flops 4031447040 | bytes 18482432 | tf_op jit(solution)/shard_map/dot_general | solution.py:27
  384.7 8.7 %reduce-scatter.2.cloned.1.call-done = f32[1024,320]{0,1:T(8,128)} async-done(((f32[2048,320]{0,1:T(8,128)}), f32[1024,320]{0,1:T(8,128)}) %reduce-scatter.2.cloned.1.call-update) | async-done | bytes 1310736 | tf_op jit(solution)/shard_map/reduce_scatter | solution.py:26
  393.4 2.4 convert_element_type.27
  395.8 6.8 %copy.15 = bf16[1536,2048]{1,0:T(8,128)(2,1)} copy(bf16[1536,2048]{1,0:T(8,128)(2,1)} %all-gather.5.cloned.1.call-done) | data formatting | bytes 12582912
  402.6 2.8 copy.16
  405.4 0.3 slice-done.3
  405.7 2.7 copy.17
  (21 shorter events, 0.1 us)
Async XLA Ops:
  7.2 2.2 copy-start.1
  7.2 2.5 copy-start.3
  7.2 14.5 %all-gather.11.cloned.1.call-start = ((), (), s32[]{:S(2)}) async-start(), calls=%async_computation.4 | async-start | bytes 1966080 | tf_op jit(solution)/shard_map/all_gather | solution.py:12
  7.9 133.3 %all-gather.5.cloned.1.call-start = ((), (), s32[]{:S(2)}) async-start(), calls=%async_computation.1 | async-start | bytes 6684672 | tf_op jit(solution)/shard_map/all_gather | solution.py:19
  9.4 2.1 copy-start.2
  10.7 247.0 %all-gather.7.cloned.1.call-start = ((), (), s32[]{:S(2)}) async-start(), calls=%async_computation.2 | async-start | bytes 6684672 | tf_op jit(solution)/shard_map/all_gather | solution.py:20
  11.4 362.7 %all-gather.9.cloned.1.call-start = ((), (), s32[]{:S(2)}) async-start(), calls=%async_computation.3 | async-start | bytes 6684672 | tf_op jit(solution)/shard_map/all_gather | solution.py:21
  12.4 381.0 %reduce-scatter.2.cloned.1.call-start = ((), (), s32[]{:S(2)}) async-start(), calls=%async_computation.5 | async-start | bytes 3932160 | tf_op jit(solution)/shard_map/reduce_scatter | solution.py:26
  23.4 350.7 %copy-start = (bf16[320,2048]{1,0:T(8,128)(2,1)S(1)}, bf16[320,2048]{1,0:T(8,128)(2,1)}, u32[]{:S(2)}) copy-start(bf16[320,2048]{1,0:T(8,128)(2,1)} %all-gather.11.cloned.1.call-done) | copy-start | bytes 3932164
  393.4 9.2 %slice-start = ((s8[6291456]{0:T(1024)(128)(4,1)}), s8[4194304]{0:T(1024)(128)(4,1)S(1)}, s32[]{:S(2)}) async-start(s8[6291456]{0:T(1024)(128)(4,1)} %bitcast.12), calls=%async_computation.6 | async-start | bytes 8388608
  395.8 6.8 %slice-start.1 = ((s8[6291456]{0:T(1024)(128)(4,1)}), s8[2097152]{0:T(1024)(128)(4,1)S(1)}, s32[]{:S(2)}) async-start(s8[6291456]{0:T(1024)(128)(4,1)} %bitcast.12), calls=%async_computation.7 | async-start | bytes 4194304
  395.8 9.6 %slice-start.2 = ((s8[6291456]{0:T(1024)(128)(4,1)}), s8[4194304]{0:T(1024)(128)(4,1)S(1)}, s32[]{:S(2)}) async-start(s8[6291456]{0:T(1024)(128)(4,1)} %bitcast.14), calls=%async_computation.8 | async-start | bytes 8388608
  402.6 3.1 slice-start.3
Sparse Core Ops, SparseCore 0:
  9.5 12.1 all-gather.10
  25.0 116.1 all-gather.4
  144.5 113.1 all-gather.6
  260.9 113.1 all-gather.8
  384.9 8.4 reduce-scatter.1
where the time goes:
time: 415 us
  waiting for transfers between devices  365 us (88%)
  matrix products  16 us (4%)
  local copies, waits for them, and re-layouts  15.2 us (4%)
  between operations  13.9 us (3%)
  other arithmetic  5.08 us (1%)
    all_gather x1, waiting for transfers between devices, on_device(): lax.all_gather(gate_low, 'fs', axis=1, tiled=True)  118 us
    all_gather x1, waiting for transfers between devices, on_device(): lax.all_gather(down_low, 'fs', axis=1, tiled=True)  116 us
    all_gather x1, waiting for transfers between devices, on_device(): lax.all_gather(up_low, 'fs', axis=1, tiled=True)  111 us
    unnamed x22, local copies, waits for them, and re-layouts  15.2 us
    dot_general x1, matrix products, on_device(): lax.dot_general(down_new, hidden, (((0,), (1,)), ((), ())), preferred_ele...  10.6 us
    all_gather x1, waiting for transfers between devices, on_device(): whole = lax.all_gather(prompt, 'tp', axis=1, tiled=True)  9.23 us
    reduce_scatter x1, waiting for transfers between devices, on_device(): lax.psum_scatter(lax.dot_general(down_new, hidden, (((0,), (1,)), ((), ()...  8.65 us
  transfers between devices with their start and end apart: 5, of which 5 were waited for; matrix products, arithmetic and copies ran while one was open for 3% of the time, Pallas kernels for 0%

commit v1 on v0

--- a/solution.py
+++ b/solution.py
@@ -2,6 +2,11 @@
 import jax.numpy as jnp
 from jax import lax
 from jax.sharding import PartitionSpec as P
+
+
+def gathered_along(x, axis, d):
+    pieces = lax.all_gather(x, axis)
+    return jnp.concatenate(pieces, axis=d)
 
 
 def on_device(prompt, norm_gain, gate_master, up_master, down_master):
@@ -16,7 +21,7 @@
     )
     contract = (((1,), (1,)), ((), ()))
     gate_new, up_new, down_new = (
-        lax.all_gather(gate_low, "fs", axis=1, tiled=True),
+        gathered_along(gate_low, "fs", 1),
         lax.all_gather(up_low, "fs", axis=1, tiled=True),
         lax.all_gather(down_low, "fs", axis=1, tiled=True),
     )

time: 415 us -> 391 us (0.942)
  waiting for transfers between devices: 365 us -> 339 us
  local copies, waits for them, and re-layouts: 15.2 us -> 19.4 us
    all_gather x1, waiting for transfers between devices: 118 us -> 96.3 us  [gathered_along(): pieces = lax.all_gather(x, axis)]
    reshape x0 -> x1, local copies, waits for them, and re-layouts: none -> 4.69 us  [gathered_along(): return jnp.concatenate(pieces, axis=d)]
    unnamed x22 -> x19, local copies, waits for them, and re-layouts: 15.2 us -> 14.8 us
where the time goes in v1:
time: 391 us
  waiting for transfers between devices  339 us (87%)
  local copies, waits for them, and re-layouts  19.4 us (5%)
  between operations  13.9 us (4%)
  matrix products  12.9 us (3%)
  other arithmetic  5.08 us (1%)
    all_gather x1, waiting for transfers between devices, on_device(): lax.all_gather(down_low, 'fs', axis=1, tiled=True)  116 us
    all_gather x1, waiting for transfers between devices, on_device(): lax.all_gather(up_low, 'fs', axis=1, tiled=True)  107 us
    all_gather x1, waiting for transfers between devices, gathered_along(): pieces = lax.all_gather(x, axis)  96.3 us
    unnamed x19, local copies, waits for them, and re-layouts  14.8 us
    dot_general x1, matrix products, on_device(): lax.dot_general(down_new, hidden, (((0,), (1,)), ((), ())), preferred_ele...  10.6 us
    all_gather x1, waiting for transfers between devices, on_device(): whole = lax.all_gather(prompt, 'tp', axis=1, tiled=True)  9.24 us
    reduce_scatter x1, waiting for transfers between devices, on_device(): lax.psum_scatter(lax.dot_general(down_new, hidden, (((0,), (1,)), ((), ()...  8.65 us
  transfers between devices with their start and end apart: 5, of which 5 were waited for; matrix products, arithmetic and copies ran while one was open for 3% of the time, Pallas kernels for 0%

profile of v1, /device:TPU:0, one launch (start us, length us, event | category | flops | bytes accessed | tf_op | source)
XLA Modules:
  0.0 390.6 jit_solution(14921053445615602)
XLA Ops:
  7.2 0.0 all-gather.10.cloned.1.call-start
  7.2 0.7 all-gather.10.cloned.1.call-update
  7.9 0.0 all-gather.12.cloned.1.call-start
  8.0 1.4 copy.11
  9.4 0.3 copy.9
  9.7 1.0 fusion.8
  10.7 0.0 all-gather.6.cloned.1.call-start
  10.7 0.7 all-gather.6.cloned.1.call-update
  11.4 0.0 all-gather.8.cloned.1.call-start
  11.5 0.9 copy.12
  12.4 0.0 reduce-scatter.2.cloned.1.call-start
  12.5 9.2 %all-gather.10.cloned.1.call-done = bf16[320,2048]{1,0:T(8,128)(2,1)} async-done(((bf16[320,1024]{1,0:T(8,128)(2,1)}), bf16[320,2048]{1,0:T(8,128)(2,1)}) %all-gather.10.cloned.1.call-update) | async-done | bytes 1310736 | tf_op jit(solution)/shard_map/all_gather | solution.py:17
  21.7 1.7 fusion.1
  23.4 96.3 %all-gather.12.cloned.1.call-done = bf16[24576,128]{1,0:T(8,128)(2,1)} async-done(((bf16[1536,128]{1,0:T(8,128)(2,1)}), bf16[24576,128]{1,0:T(8,128)(2,1)}) %all-gather.12.cloned.1.call-update) | async-done | bytes 6291472 | tf_op jit(solution)/shard_map/all_gather | solution.py:8
  119.7 4.7 %copy.15 = bf16[16,192,8,128]{3,2,0,1:T(8,128)(2,1)S(1)} copy(bf16[16,192,8,128]{3,2,1,0:T(8,128)(2,1)} %bitcast.21) | data formatting | bytes 12582912 | tf_op jit(solution)/shard_map/reshape | solution.py:9
  124.4 2.7 copy-done
  127.1 2.2 fusion.5
  129.3 107.2 %all-gather.6.cloned.1.call-done = bf16[1536,2048]{1,0:T(8,128)(2,1)} async-done(((bf16[1536,128]{1,0:T(8,128)(2,1)}), bf16[1536,2048]{1,0:T(8,128)(2,1)}) %all-gather.6.cloned.1.call-update) | async-done | bytes 6291472 | tf_op jit(solution)/shard_map/all_gather | solution.py:25
  236.5 116.4 %all-gather.8.cloned.1.call-done = bf16[1536,2048]{1,0:T(8,128)(2,1)} async-done(((bf16[1536,128]{1,0:T(8,128)(2,1)}), bf16[1536,2048]{1,0:T(8,128)(2,1)}) %all-gather.8.cloned.1.call-update) | async-done | bytes 6291472 | tf_op jit(solution)/shard_map/all_gather | solution.py:26
  352.9 10.6 %convolution_bitcast_fusion = f32[2048,320]{0,1:T(8,128)} fusion(bf16[1536,2048]{1,0:T(8,128)(2,1)} %all-gather.8.cloned.1.call-done, bf16[1536,2048]{1,0:T(8,128)(2,1)} %all-gather.6.cloned.1.call-done, f32[320,1536]{1,0:T(8,128)S(1)} %fusion.5, bf16[320,2048]{1,0:T(8,128)(2,1)S(1)} %copy-done.1, f32[320]{0:T(512)S(1)} %add_rsqrt_fusion), kind=kOutput, calls=%fused_computation.4 | convolution fusion | flops 4031447040 | bytes 18482432 | tf_op jit(solution)/shard_map/dot_general | solution.py:32
  363.6 8.7 %reduce-scatter.2.cloned.1.call-done = f32[1024,320]{0,1:T(8,128)} async-done(((f32[2048,320]{0,1:T(8,128)}), f32[1024,320]{0,1:T(8,128)}) %reduce-scatter.2.cloned.1.call-update) | async-done | bytes 1310736 | tf_op jit(solution)/shard_map/reduce_scatter | solution.py:31
  372.2 2.4 convert_element_type.27
  374.6 6.8 %copy.18 = bf16[1536,2048]{1,0:T(8,128)(2,1)} copy(bf16[1536,2048]{1,0:T(8,128)(2,1)} %all-gather.6.cloned.1.call-done) | data formatting | bytes 12582912
  381.4 2.7 copy.19
  (18 shorter events, 0.1 us)
Async XLA Ops:
  7.2 2.2 copy-start.2
  7.2 2.5 copy-start.4
  7.2 14.5 %all-gather.10.cloned.1.call-start = ((), (), s32[]{:S(2)}) async-start(), calls=%async_computation.3 | async-start | bytes 1966080 | tf_op jit(solution)/shard_map/all_gather | solution.py:17
  7.9 111.7 %all-gather.12.cloned.1.call-start = ((), (), s32[]{:S(2)}) async-start(), calls=%async_computation.5 | async-start | bytes 6684672 | tf_op jit(solution)/shard_map/all_gather | solution.py:8
  9.4 2.1 copy-start.3
  10.7 225.9 %all-gather.6.cloned.1.call-start = ((), (), s32[]{:S(2)}) async-start(), calls=%async_computation.1 | async-start | bytes 6684672 | tf_op jit(solution)/shard_map/all_gather | solution.py:25
  11.4 341.5 %all-gather.8.cloned.1.call-start = ((), (), s32[]{:S(2)}) async-start(), calls=%async_computation.2 | async-start | bytes 6684672 | tf_op jit(solution)/shard_map/all_gather | solution.py:26
  12.4 359.8 %reduce-scatter.2.cloned.1.call-start = ((), (), s32[]{:S(2)}) async-start(), calls=%async_computation.4 | async-start | bytes 3932160 | tf_op jit(solution)/shard_map/reduce_scatter | solution.py:31
  119.7 7.4 %copy-start.1 = (bf16[320,2048]{1,0:T(8,128)(2,1)S(1)}, bf16[320,2048]{1,0:T(8,128)(2,1)}, u32[]{:S(2)}) copy-start(bf16[320,2048]{1,0:T(8,128)(2,1)} %all-gather.10.cloned.1.call-done) | copy-start | bytes 3932164
  124.4 2.7 copy-start
  372.2 9.2 %slice-start = ((s8[6291456]{0:T(1024)(128)(4,1)}), s8[4194304]{0:T(1024)(128)(4,1)S(1)}, s32[]{:S(2)}) async-start(s8[6291456]{0:T(1024)(128)(4,1)} %bitcast.19), calls=%async_computation.6 | async-start | bytes 8388608
  374.6 6.8 %slice-start.1 = ((s8[6291456]{0:T(1024)(128)(4,1)}), s8[2097152]{0:T(1024)(128)(4,1)S(1)}, s32[]{:S(2)}) async-start(s8[6291456]{0:T(1024)(128)(4,1)} %bitcast.19), calls=%async_computation.7 | async-start | bytes 4194304
Sparse Core Ops, SparseCore 0:
  9.5 12.1 all-gather.9
  25.1 94.5 all-gather.11
  122.9 113.5 all-gather.5
  239.7 113.1 all-gather.7
  363.7 8.4 reduce-scatter.1
